TPU v7x, 256 devices: a whole 4x4x8 slice. The times are simulated.
256 devices in a mesh: sp: 64 (over z, y, core), tp: 4 (over x).
Axes of the slice: x: 4, y: 4, z: 8, core: 2. Of those that a mesh axis runs over, the one named last changes fastest.
Arguments:
- head_queries: bfloat16 [16384, 2048], P('sp', 'tp'), may hold values from -6 to 6
- head_keys: bfloat16 [16384, 2048], P('sp', 'tp'), may hold values from -6 to 6
- head_values: bfloat16 [16384, 2048], P('sp', 'tp'), may hold values from -6 to 6
- decay_logits: bfloat16 [16384, 2048], P('sp', 'tp'), may hold values from -12 to 1
- learning_logits: bfloat16 [16384, 32], P('sp', 'tp'), may hold values from -9 to 2
- surge_decay: float32 [16384, 32], P('sp', 'tp'), may hold values from -0.7 to 0
- documents: int32 [16384], P('sp'), may hold values from 0 to 16, never falling along the last dimension, each value on 1 to 1536 neighbouring positions
- residual: bfloat16 [16384, 2048], P(('sp', 'tp')), may hold values from -6 to 6
- head_norm_scale: float32 [2048], P('tp'), may hold values from 0.1 to 1.9
- mixer_output_weight: bfloat16 [2048, 2048], P('tp'), may hold values from -0.125 to 0.125
- layer_norm_scale: float32 [2048], replicated, may hold values from 0.1 to 1.9
- routes: int32 [16384, 2], P('sp'), may hold values from 0 to 127, all different within a row; in each aligned block of 64 rows (0 to 63, 64 to 127, ...) at most 2 rows name the same one
- routing_weight: float32 [16384, 2], P(('sp', 'tp')), may hold values from 0.3 to 1.5
- routed_gate_weight: bfloat16 [128, 2048, 1024], P('sp', None, 'tp'), may hold values from -0.125 to 0.125
- routed_up_weight: bfloat16 [128, 2048, 1024], P('sp', None, 'tp'), may hold values from -0.125 to 0.125
- routed_down_weight: bfloat16 [128, 1024, 2048], P('sp', 'tp'), may hold values from -0.1875 to 0.1875
- common_gate_weight: bfloat16 [2048, 512], P(None, 'tp'), may hold values from -0.125 to 0.125
- common_up_weight: bfloat16 [2048, 512], P(None, 'tp'), may hold values from -0.125 to 0.125
- common_down_weight: bfloat16 [512, 2048], P('tp'), may hold values from -0.25 to 0.25
Outputs:
- layer_out: bfloat16 [16384, 2048], P(('sp', 'tp'))
Inputs may be any that keep to these rules, and one draw needn't show every extreme that they name: `documents`: numbers never fall along the positions; each document holds 1 to 1536 positions and one holds exactly 1536. `routes`: each row names 2 different experts; in each aligned block of 64 rows no expert is named by more than 2 rows, a bound that some block reaches.
All inputs are finite; a program needn't handle non-finite values.
Results may differ from a plain program's by a relative error of at most 0.019.
Values may be sent and summed in bfloat16 or wider, within the bound.
A program may use at most 128 MiB of HBM per device.

v0:
```python
import jax
import jax.numpy as jnp
from jax import lax
from jax.sharding import Mesh
from jax.sharding import PartitionSpec as P

HEAD = 64
EXP_DEV = 2
TOP = 2
BLOCK_SPAN = 64
TOK_DEV = 64
SP = ("sp_0", "sp_1", "sp_2")
SP_TP = ("sp_0", "sp_1", "sp_2", "tp")
residual_scale = 2.0**0.5
group_eps = 0.00064
norm_eps = 1e-05
unit_eps = 1e-06
highest = lax.Precision.HIGHEST


def filled_with(x, identity):
    return jax.tree.map(
        lambda a, e: jnp.broadcast_to(jnp.asarray(e, a.dtype), a.shape), x, identity
    )


def all_in_one(x, axis):
    leaves = jax.tree.leaves(x)
    order = sorted(range(len(leaves)), key=lambda k: -leaves[k].size)
    width = (1, *leaves[order[0]].shape)[-1]
    lines = [
        jnp.pad(leaves[k].reshape(-1), (0, -leaves[k].size % width)).reshape(-1, width)
        for k in order
    ]
    both, at, found = (lax.all_gather(jnp.concatenate(lines), axis), 0, {})
    for k, line in zip(order, lines):
        piece = both[:, at : at + len(line)].reshape(len(both), -1)
        found[k] = piece[:, : leaves[k].size].reshape(-1, *leaves[k].shape)
        at += len(line)
    numbers = iter(range(len(leaves)))
    return jax.tree.map(lambda _: found[next(numbers)], x)


def prefix_by_axis(x, axes, combine, identity):
    before = start = filled_with(x, identity)
    running = x
    for axis in reversed(axes):
        devices, position = (lax.axis_size(axis), lax.axis_index(axis))
        pieces = all_in_one(
            jax.tree.map(
                lambda part, kind: part.astype(kind),
                running,
                (jnp.bfloat16, jnp.bfloat16, jnp.bfloat16, jnp.bfloat16),
            ),
            axis,
        )
        inside, running = (start, start)
        for k in range(devices):
            passed = k < position
            running = combine(
                running, jax.tree.map(lambda part, own: part[k].astype(own.dtype), pieces, x)
            )
            inside = jax.tree.map(lambda new, old: jnp.where(passed, new, old), running, inside)
        before = combine(inside, before)
    return before


def split_up(x, dim, devices):
    shape = x.shape
    pieces = x.reshape(*shape[:dim], devices, shape[dim] // devices, *shape[dim + 1 :])
    return jnp.moveaxis(pieces, dim, 0)


def sent_and_summed(x, axis, dim):
    pieces = split_up(x, dim, lax.axis_size(axis))
    arrived = lax.all_to_all(pieces, axis, split_axis=0, concat_axis=0, tiled=True)
    return arrived.astype(jnp.float32).sum(axis=0)


def pair_scores(left, right):
    return jnp.einsum("bhtn,bhsn->bhts", left, right, precision=highest)


def apply_scores(scores, operand):
    return jnp.einsum("bhts,bhsn->bhtn", scores, operand, precision=highest)


def split_heads(values, block_list, head_number):
    return (
        values.astype(jnp.float32)
        .reshape(block_list, BLOCK_SPAN, head_number, HEAD)
        .transpose(0, 2, 1, 3)
    )


def unit_lower_inverse(strict_part):
    power = strict_part
    inverse = jnp.eye(BLOCK_SPAN, dtype=jnp.float32) - strict_part
    reach = 2
    while reach < BLOCK_SPAN:
        power = apply_scores(power, power)
        inverse = inverse + apply_scores(inverse, power)
        reach = reach * 2
    return inverse


def link_states(earlier, later):
    map_one, add_one, first_one, last_one = earlier
    map_two, add_two, first_two, last_two = later
    joined = ((last_one == first_two) | (last_one < 0) | (first_two < 0)).astype(jnp.float32)
    map_out = joined * jnp.einsum("hij,hjk->hik", map_one, map_two, precision=highest)
    add_out = joined * jnp.einsum("hij,hjk->hik", add_one, map_two, precision=highest) + add_two
    first_out = jnp.where(first_one < 0, first_two, first_one)
    last_out = jnp.where(last_two < 0, last_one, last_two)
    return (map_out, add_out, first_out, last_out)


def linear_recurrence_mixer(
    head_queries,
    head_keys,
    head_values,
    decay_logits,
    learning_logits,
    surge_decay,
    documents,
    head_norm_scale,
):
    length, local_width = head_queries.shape
    head_number = local_width // HEAD
    block_list = length // BLOCK_SPAN
    read_heads = split_heads(head_queries, block_list, head_number)
    key_heads = split_heads(head_keys, block_list, head_number)
    values = split_heads(head_values, block_list, head_number)
    unit_keys = key_heads * lax.rsqrt(jnp.sum(key_heads * key_heads, -1, keepdims=True) + unit_eps)
    learn_rate = (
        jax.nn.sigmoid(learning_logits.astype(jnp.float32))
        .reshape(block_list, BLOCK_SPAN, head_number)
        .transpose(0, 2, 1)
    )
    surge_list = surge_decay.reshape(block_list, BLOCK_SPAN, head_number).transpose(0, 2, 1)
    decay_logarithm = split_heads(
        -jnp.exp(-jax.nn.softplus(-decay_logits.astype(jnp.float32)) - 0.5), block_list, head_number
    )
    decay_logarithm = decay_logarithm + surge_list[..., None]
    cumulative = jnp.cumsum(decay_logarithm, axis=2)
    before = cumulative - decay_logarithm
    doc_blocks = documents.reshape(block_list, BLOCK_SPAN)
    prior_doc = jnp.concatenate([doc_blocks[:1, 0], doc_blocks[:-1, -1]])
    joined = (doc_blocks == prior_doc[:, None]).astype(jnp.float32)[:, None, :, None]
    same_doc = doc_blocks[:, :, None] == doc_blocks[:, None, :]
    later_pos = lax.broadcasted_iota(jnp.int32, (BLOCK_SPAN, BLOCK_SPAN), 0)
    earlier_pos = lax.broadcasted_iota(jnp.int32, (BLOCK_SPAN, BLOCK_SPAN), 1)
    strict = (same_doc & (later_pos > earlier_pos)[None]).astype(jnp.float32)[:, None]
    causal_incl = (same_doc & (later_pos >= earlier_pos)[None]).astype(jnp.float32)[:, None]
    ahead_unit = unit_keys * jnp.exp(before)
    back_unit = unit_keys * jnp.exp(-cumulative)
    back_key = key_heads * jnp.exp(-cumulative)
    forward = read_heads * jnp.exp(cumulative)
    lower_part = pair_scores(ahead_unit, back_unit) * strict * learn_rate[:, :, None, :]
    mix_key = pair_scores(ahead_unit, back_key) * strict
    right_side = jnp.concatenate([ahead_unit * joined, apply_scores(mix_key, values)], -1)
    solved = apply_scores(unit_lower_inverse(lower_part), right_side)
    carry_map = solved[..., :HEAD]
    local_pull = solved[..., HEAD:]
    read_unit = pair_scores(forward, back_unit) * causal_incl * -learn_rate[:, :, None, :]
    read_key = pair_scores(forward, back_key) * causal_incl
    local_out = apply_scores(read_unit, local_pull) + apply_scores(read_key, values)
    read_start = forward * joined + apply_scores(read_unit, carry_map)
    block_total = cumulative[:, :, -1:, :]
    tail_mask = (doc_blocks == doc_blocks[:, -1:]).astype(jnp.float32)[:, None, :, None]
    end_unit = unit_keys * jnp.exp(block_total - cumulative) * tail_mask * -learn_rate[..., None]
    end_key = key_heads * jnp.exp(block_total - cumulative) * tail_mask
    block_map = jnp.eye(HEAD, dtype=jnp.float32) * (jnp.exp(block_total) * joined[:, :, -1:, :])
    block_map = block_map + jnp.einsum("bhsn,bhsm->bhnm", carry_map, end_unit, precision=highest)
    block_add = jnp.einsum("bhsv,bhsm->bhvm", local_pull, end_unit, precision=highest)
    block_add = block_add + jnp.einsum("bhsv,bhsm->bhvm", values, end_key, precision=highest)
    identity_map = jnp.broadcast_to(jnp.eye(HEAD, dtype=jnp.float32), (head_number, HEAD, HEAD))
    carried = jnp.zeros((head_number, HEAD, HEAD), jnp.float32)
    through = identity_map
    outputs = []
    starts = []
    for block_index in range(block_list):
        outputs.append(
            local_out[block_index]
            + jnp.einsum("hlm,hvm->hlv", read_start[block_index], carried, precision=highest)
        )
        starts.append(
            jnp.einsum("hlm,hnm->hln", read_start[block_index], through, precision=highest)
        )
        carried = (
            jnp.einsum("hvn,hnm->hvm", carried, block_map[block_index], precision=highest)
            + block_add[block_index]
        )
        through = jnp.einsum("hvn,hnm->hvm", through, block_map[block_index], precision=highest)
    first_doc = documents[0].astype(jnp.float32)
    last_doc = documents[-1].astype(jnp.float32)
    no_doc = jnp.full((), -1.0, jnp.float32)
    identity = (identity_map, jnp.zeros((head_number, HEAD, HEAD), jnp.float32), no_doc, no_doc)
    prefix = prefix_by_axis((through, carried, first_doc, last_doc), SP, link_states, identity)
    incoming = prefix[1] * (prefix[3] == first_doc).astype(jnp.float32)
    head_read = jnp.stack(outputs) + jnp.einsum(
        "bhln,hvn->bhlv", jnp.stack(starts), incoming, precision=highest
    )
    centre = jnp.mean(head_read, -1, keepdims=True)
    spread = jnp.mean(jnp.square(head_read - centre), -1, keepdims=True)
    normed = (
        ((head_read - centre) * lax.rsqrt(spread + group_eps))
        .transpose(0, 2, 1, 3)
        .reshape(length, local_width)
    )
    return (normed * head_norm_scale).astype(jnp.bfloat16)


def per_device(
    head_queries,
    head_keys,
    head_values,
    decay_logits,
    learning_logits,
    surge_decay,
    documents,
    residual,
    head_norm_scale,
    mixer_output_weight,
    layer_norm_scale,
    routes,
    routing_weight,
    routed_gate_weight,
    routed_up_weight,
    routed_down_weight,
    common_gate_weight,
    common_up_weight,
    common_down_weight,
):
    head_outputs = linear_recurrence_mixer(
        head_queries,
        head_keys,
        head_values,
        decay_logits,
        learning_logits,
        surge_decay,
        documents,
        head_norm_scale,
    )
    mixed_rows = sent_and_summed(
        jnp.dot(head_outputs, mixer_output_weight, preferred_element_type=jnp.float32).astype(
            jnp.bfloat16
        ),
        "tp",
        0,
    )
    summed = residual_scale * residual.astype(jnp.float32) + mixed_rows
    centre = jnp.mean(summed, -1, keepdims=True)
    spread = jnp.mean(jnp.square(summed - centre), -1, keepdims=True)
    stream = ((summed - centre) * lax.rsqrt(spread + norm_eps) * layer_norm_scale).astype(
        jnp.bfloat16
    )
    quarters = lax.axis_size("tp")
    groups = lax.axis_size(SP)
    experts = EXP_DEV * groups
    capacity = max(2, (3 * TOK_DEV * TOP + 2 * experts - 1) // (2 * experts))
    own_rows, model_width = stream.shape
    chosen = routes.reshape(quarters, own_rows * TOP)
    onehot = (chosen[..., None] == jnp.arange(experts, dtype=jnp.int32)).astype(jnp.int32)
    ranking = jnp.sum(jnp.cumsum(onehot, 1) * onehot, -1) - 1
    slot_index = chosen * capacity + ranking
    own_slots = lax.dynamic_index_in_dim(slot_index, lax.axis_index("tp"), 0, keepdims=False)
    outgoing = jnp.zeros((experts * capacity, model_width), jnp.bfloat16)
    outgoing = outgoing.at[own_slots].set(jnp.repeat(stream, TOP, axis=0))
    arrived = lax.all_to_all(
        outgoing.reshape(groups, EXP_DEV, capacity, model_width),
        SP,
        split_axis=0,
        concat_axis=0,
        tiled=True,
    )
    arrived_all, rows_all = (
        lax.all_gather(arrived[None], "tp", axis=0, tiled=True),
        lax.all_gather(stream, "tp", axis=0, tiled=True),
    )
    gated = jnp.einsum(
        "qsecd,edf->qsecf", arrived_all, routed_gate_weight, preferred_element_type=jnp.float32
    )
    lifted = jnp.einsum(
        "qsecd,edf->qsecf", arrived_all, routed_up_weight, preferred_element_type=jnp.float32
    )
    hidden = (jax.nn.silu(gated) * lifted).astype(jnp.bfloat16)
    partial_value = jnp.einsum(
        "qsecf,efd->qsecd", hidden, routed_down_weight, preferred_element_type=jnp.float32
    )
    shared_gated = jnp.dot(rows_all, common_gate_weight, preferred_element_type=jnp.float32)
    shared_lifted = jnp.dot(rows_all, common_up_weight, preferred_element_type=jnp.float32)
    shared_hidden = (jax.nn.silu(shared_gated) * shared_lifted).astype(jnp.bfloat16)
    shared_part = jnp.dot(shared_hidden, common_down_weight, preferred_element_type=jnp.float32)
    expert_sum, shared_sum = (
        sent_and_summed(partial_value.astype(jnp.bfloat16), "tp", 0),
        sent_and_summed(shared_part.astype(jnp.bfloat16), "tp", 0),
    )
    returned = lax.all_to_all(
        expert_sum[0].astype(jnp.bfloat16), SP, split_axis=0, concat_axis=0, tiled=True
    )
    picked = returned.reshape(experts * capacity, model_width)[own_slots]
    weighted = (
        picked.astype(jnp.float32).reshape(own_rows, TOP, model_width) * routing_weight[:, :, None]
    )
    routed = jnp.sum(weighted, 1)
    return (residual_scale * stream.astype(jnp.float32) + routed + shared_sum).astype(jnp.bfloat16)


def solution(mesh):
    torus = Mesh(mesh.devices.reshape(8, 4, 2, mesh.shape["tp"]), ("sp_0", "sp_1", "sp_2", "tp"))
    placed = (
        P(SP, "tp"),
        P(SP, "tp"),
        P(SP, "tp"),
        P(SP, "tp"),
        P(SP, "tp"),
        P(SP, "tp"),
        P(SP),
        P(SP_TP, None),
        P("tp"),
        P("tp", None),
        P(),
        P(SP, None),
        P(SP_TP, None),
        P(SP, None, "tp"),
        P(SP, None, "tp"),
        P(SP, "tp", None),
        P(None, "tp"),
        P(None, "tp"),
        P("tp", None),
    )
    return jax.shard_map(
        per_device, mesh=torus, in_specs=placed, out_specs=P(SP_TP, None), check_vma=False
    )
```

profile of v0, /device:TPU:1, one launch (start us, length us, event | category | flops | bytes accessed | tf_op | source)
XLA Modules:
  0.0 536.4 jit_solution(10089789795744124520)
XLA Ops:
  14.4 2.3 reshape.498
  22.5 3.1 convolution_multiply_fusion.1
  25.6 2.2 fusion.17
  35.1 12.9 %convolution_add_fusion.2 = f32[4,8,64,64]{3,2,1,0:T(8,128)S(1)} fusion(f32[4,8,64,64]{3,2,1,0:T(8,128)S(1)} %convolution_add_fusion.3, f32[4,8,64,64]{3,2,1,0:T(8,128)S(1)} %fusion.188), kind=kOutput, calls=%fused_computation.17 | convolution fusion | flops 100794368 | bytes 1572864 | tf_op jit(solution)/shard_map/bhts,bhsn->bhtn/dot_general | solution.py:85
  48.0 2.2 fusion.190
  50.2 2.2 convolution_add_fusion.1
  53.8 3.2 convolution_add_fusion
  60.7 3.0 convolution_add_fusion.5
  63.7 2.5 convolution_add_fusion.6
  72.0 2.1 convolution_convert_fusion.2
  81.6 5.0 all-gather.4
  102.9 2.0 convolution_add_fusion.12
  107.4 2.1 fusion.182
  110.5 2.0 fusion.181
  115.7 10.6 %all-gather.5 = bf16[4,1026,64]{1,2,0:T(8,128)(2,1)S(1)} all-gather(bf16[1,1026,64]{1,2,0:T(8,128)(2,1)} %bitcast.420), channel_id=3, replica_groups=mesh['sp_0'=8,'sp_1'=4,'sp_2'=2,'tp'=4] {'sp_1'}, dimensions={0}, use_global_device_ids=true | all-gather | bytes 656640 | tf_op jit(solution)/shard_map/all_gather | solution.py:35
  149.5 2.0 convolution_add_fusion.11
  164.7 2.1 fusion.184
  171.6 1.9 fusion.183
  176.8 2.2 reshape.578
  178.9 4.2 fusion.18
  183.2 3.4 convolution_multiply_fusion
  186.5 3.1 fusion.80
  196.6 2.3 convolution_bitcast_fusion.2
  198.9 2.6 convolution_add_fusion.8
  209.4 5.8 %all-gather.15.cloned.1.call-done = bf16[8,1026,64]{1,2,0:T(8,128)(2,1)} async-done(((bf16[1,1026,64]{1,2,0:T(8,128)(2,1)}), bf16[8,1026,64]{1,2,0:T(8,128)(2,1)}) %all-gather.15.cloned.1.call-update) | async-done | bytes 1050640 | tf_op jit(solution)/shard_map/all_gather | solution.py:35
  237.1 2.1 fusion.172
  259.4 3.1 fusion.185
  266.1 3.3 convolution_convert_fusion.1
  269.4 4.3 all-to-all-start
  274.8 1.9 reduce_window_sum.23
  278.0 5.5 %all-to-all-done = bf16[4,64,2048]{2,1,0:T(8,128)(2,1)S(1)} async-done(((bf16[4,64,2048]{2,1,0:T(8,128)(2,1)}), bf16[4,64,2048]{2,1,0:T(8,128)(2,1)S(1)}, u32[]{:S(2)}, u32[]{:S(2)}) %all-to-all-start) | async-done | bytes 1048608 | tf_op jit(solution)/shard_map/all_to_all | solution.py:76
  285.9 2.2 scatter_custom_fusion
  289.6 42.3 %all_to_all.25 = bf16[64,2,2,2048]{3,2,1,0:T(2,128)(2,1)} all-to-all(bf16[64,2,2,2048]{3,2,1,0:T(2,128)(2,1)} %reshape.531), channel_id=1, replica_groups=mesh['sp_0'=8,'sp_1'=4,'sp_2'=2,'tp'=4] {'sp_0','sp_1','sp_2'}, dimensions={0} | all-to-all | bytes 2097152 | tf_op jit(solution)/shard_map/all_to_all | solution.py:270
  331.9 45.8 %all-gather.13.cloned.1.call-done = bf16[256,2,2,2048]{3,2,1,0:T(2,128)(2,1)} async-done(((bf16[64,2,2,2048]{3,2,1,0:T(2,128)(2,1)}), bf16[256,2,2,2048]{3,2,1,0:T(2,128)(2,1)}) %all-gather.13.cloned.1.call-update) | async-done | bytes 4194320 | tf_op jit(solution)/shard_map/all_gather | solution.py:278
  377.7 4.6 copy.284
  382.3 2.0 copy-done.17
  385.6 7.3 %convert_bitcast_fusion = bf16[4,1,64,2,2,2048]{5,2,4,0,3,1:T(8,128)(2,1)} fusion(bf16[2,256,2048]{2,1,0:T(8,128)(2,1)S(1)} %copy-done, bf16[2,2048,256]{2,1,0:T(8,128)(2,1)} %param.33, bf16[4,64,2,2,2048]{4,1,0,3,2:T(8,128)(2,1)} %bitcast.391, f32[4,64,2,2,256]{4,1,3,0,2:T(8,128)S(1)} %fusion.7), kind=kOutput, calls=%fused_computation.2 | convolution fusion | flops 2151153664 | bytes 13631488 | tf_op jit(solution)/shard_map/qsecf,efd->qsecd/dot_general | solution.py:288
  392.9 4.8 copy.287
  397.7 4.9 all-to-all-start.2
  403.3 36.8 %all-gather.11.cloned.1.call-done = bf16[256,2048]{1,0:T(8,128)(2,1)} async-done(((bf16[64,2048]{1,0:T(8,128)(2,1)}), bf16[256,2048]{1,0:T(8,128)(2,1)}) %all-gather.11.cloned.1.call-update) | async-done | bytes 1048592 | tf_op jit(solution)/shard_map/all_gather | solution.py:279
  441.9 2.9 convolution_convert_fusion
  444.9 14.2 %all-to-all-done.2 = bf16[4,1,64,2,2,2048]{5,2,4,3,1,0:T(8,128)(2,1)} async-done(((bf16[4,1,64,2,2,2048]{5,2,4,3,1,0:T(8,128)(2,1)}), bf16[4,1,64,2,2,2048]{5,2,4,3,1,0:T(8,128)(2,1)}, u32[]{:S(2)}, u32[]{:S(2)}) %all-to-all-start.2) | async-done | bytes 4194336 | tf_op jit(solution)/shard_map/all_to_all | solution.py:76
  459.1 7.8 %all-to-all-start.4 = ((bf16[4,64,2048]{2,1,0:T(8,128)(2,1)}), bf16[4,64,2048]{2,1,0:T(8,128)(2,1)S(1)}, u32[]{:S(2)}, u32[]{:S(2)}) async-start(bf16[4,64,2048]{2,1,0:T(8,128)(2,1)} %bitcast.137), calls=%async_computation.4 | async-start | bytes 2097152 | tf_op jit(solution)/shard_map/all_to_all | solution.py:76
  466.9 4.3 reduce_sum.100
  471.2 3.3 copy.289
  474.5 6.7 %all-to-all-done.4 = bf16[4,64,2048]{2,1,0:T(8,128)(2,1)S(1)} async-done(((bf16[4,64,2048]{2,1,0:T(8,128)(2,1)}), bf16[4,64,2048]{2,1,0:T(8,128)(2,1)S(1)}, u32[]{:S(2)}, u32[]{:S(2)}) %all-to-all-start.4) | async-done | bytes 1048608 | tf_op jit(solution)/shard_map/all_to_all | solution.py:76
  481.2 11.9 %all-to-all-start.3 = ((bf16[64,2,2,2048]{3,2,1,0:T(2,128)(2,1)}), bf16[64,2,2,2048]{3,2,1,0:T(2,128)(2,1)}, u32[]{:S(2)}, u32[]{:S(2)}) async-start(bf16[64,2,2,2048]{3,2,1,0:T(2,128)(2,1)} %copy.289), calls=%async_computation.3 | async-start | bytes 2097152 | tf_op jit(solution)/shard_map/all_to_all | solution.py:299
  494.2 27.0 %all-to-all-done.3 = bf16[64,2,2,2048]{3,2,1,0:T(2,128)(2,1)} async-done(((bf16[64,2,2,2048]{3,2,1,0:T(2,128)(2,1)}), bf16[64,2,2,2048]{3,2,1,0:T(2,128)(2,1)}, u32[]{:S(2)}, u32[]{:S(2)}) %all-to-all-start.3) | async-done | bytes 1048608 | tf_op jit(solution)/shard_map/all_to_all | solution.py:299
  (324 shorter events, 145.6 us)
Async XLA Ops:
  6.5 379.0 %copy-start = (bf16[2,256,2048]{2,1,0:T(8,128)(2,1)S(1)}, bf16[2,256,2048]{2,1,0:T(8,128)(2,1)}, u32[]{:S(2)}) copy-start(bf16[2,256,2048]{2,1,0:T(8,128)(2,1)} %param.34) | copy-start | bytes 6291460
  6.5 6.6 %copy-start.71 = (bf16[256,8]{0,1:T(8,128)(2,1)S(1)}, bf16[256,8]{0,1:T(8,128)(2,1)}, u32[]{:S(2)}) copy-start(bf16[256,8]{0,1:T(8,128)(2,1)} %param.23) | copy-start | bytes 12292
  6.5 6.7 %copy-start.57 = (bf16[256,512]{1,0:T(8,128)(2,1)S(1)}, bf16[256,512]{1,0:T(8,128)(2,1)}, u32[]{:S(2)}) copy-start(bf16[256,512]{1,0:T(8,128)(2,1)} %param.22) | copy-start | bytes 786436
  6.5 208.6 %all-gather.15.cloned.1.call-start = ((), (), s32[]{:S(2)}) async-start(), calls=%async_computation.7 | async-start | bytes 1327104 | tf_op jit(solution)/shard_map/all_gather | solution.py:35
  12.7 4.1 copy-start.1
  12.7 4.0 copy-start.70
  16.8 3.8 copy-start.10
  53.5 3.5 copy-start.12
  53.5 3.5 copy-start.19
  66.2 3.8 copy-start.11
  66.5 3.4 copy-start.21
  178.9 4.2 copy-start.4
  178.9 4.2 copy-start.7
  178.9 4.2 copy-start.43
  183.2 3.4 copy-start.6
  191.3 5.3 copy-start.20
  191.3 7.6 %copy-start.13 = (bf16[4,64,8,64]{3,2,1,0:T(8,128)(2,1)S(1)}, bf16[4,64,8,64]{3,2,1,0:T(8,128)(2,1)}, u32[]{:S(2)}) copy-start(bf16[4,64,8,64]{3,2,1,0:T(8,128)(2,1)} %reshape.502) | copy-start | bytes 786436
  196.6 5.0 copy-start.9
  198.9 4.0 copy-start.31
  198.9 5.2 copy-start.41
  201.5 3.9 copy-start.29
  201.6 5.1 copy-start.42
  201.6 5.1 copy-start.47
  202.9 4.2 copy-start.24
  202.9 4.2 copy-start.27
  202.9 4.2 copy-start.34
  202.9 4.2 copy-start.49
  204.1 4.1 copy-start.32
  204.1 4.1 copy-start.36
  204.1 4.1 copy-start.39
  204.1 4.1 copy-start.50
  252.9 3.8 copy-start.53
  252.9 4.1 copy-start.54
  252.9 4.3 copy-start.55
  254.2 3.3 copy-start.44
  254.2 3.3 copy-start.56
  266.0 7.7 %copy-start.73 = (s32[256,2]{0,1:T(2,128)S(1)}, s32[256,2]{0,1:T(2,128)}, u32[]{:S(2)}) copy-start(s32[256,2]{0,1:T(2,128)} %param.30) | copy-start | bytes 6148
  269.4 14.2 %copy-start.25 = (bf16[64,2048]{1,0:T(8,128)(2,1)S(1)}, bf16[64,2048]{1,0:T(8,128)(2,1)}, u32[]{:S(2)}) copy-start(bf16[64,2048]{1,0:T(8,128)(2,1)} %param.26) | copy-start | bytes 786436
  269.4 14.1 %all-to-all-start = ((bf16[4,64,2048]{2,1,0:T(8,128)(2,1)}), bf16[4,64,2048]{2,1,0:T(8,128)(2,1)S(1)}, u32[]{:S(2)}, u32[]{:S(2)}) async-start(bf16[4,64,2048]{2,1,0:T(8,128)(2,1)} %bitcast.123), calls=%async_computation | async-start | bytes 2097152 | tf_op jit(solution)/shard_map/all_to_all | solution.py:76
  273.7 104.0 %all-gather.13.cloned.1.call-start = ((), (), s32[]{:S(2)}) async-start(), calls=%async_computation.6 | async-start | bytes 5242880 | tf_op jit(solution)/shard_map/all_gather | solution.py:278
  274.0 10.0 %copy-start.69 = (f32[2048]{0:T(1024)S(1)}, f32[2048]{0:T(1024)}, u32[]{:S(2)}) copy-start(f32[2048]{0:T(1024)} %param.29) | copy-start | bytes 24580
  284.5 5.1 copy-start.15
  377.7 6.6 %copy-start.77 = (bf16[2,2048,256]{2,1,0:T(8,128)(2,1)S(1)}, bf16[2,2048,256]{2,1,0:T(8,128)(2,1)}, u32[]{:S(2)}) copy-start(bf16[2,2048,256]{2,1,0:T(8,128)(2,1)} %param.32) | copy-start | bytes 6291460
  397.7 61.4 %all-to-all-start.2 = ((bf16[4,1,64,2,2,2048]{5,2,4,3,1,0:T(8,128)(2,1)}), bf16[4,1,64,2,2,2048]{5,2,4,3,1,0:T(8,128)(2,1)}, u32[]{:S(2)}, u32[]{:S(2)}) async-start(bf16[4,1,64,2,2,2048]{5,2,4,3,1,0:T(8,128)(2,1)} %copy.287), calls=%async_computation.2 | async-start | bytes 8388608 | tf_op jit(solution)/shard_map/all_to_all | solution.py:76
  402.6 37.5 %all-gather.11.cloned.1.call-start = ((), (), s32[]{:S(2)}) async-start(), calls=%async_computation.5 | async-start | bytes 1310720 | tf_op jit(solution)/shard_map/all_gather | solution.py:279
  459.1 22.1 %all-to-all-start.4 = ((bf16[4,64,2048]{2,1,0:T(8,128)(2,1)}), bf16[4,64,2048]{2,1,0:T(8,128)(2,1)S(1)}, u32[]{:S(2)}, u32[]{:S(2)}) async-start(bf16[4,64,2048]{2,1,0:T(8,128)(2,1)} %bitcast.137), calls=%async_computation.4 | async-start | bytes 2097152 | tf_op jit(solution)/shard_map/all_to_all | solution.py:76
  471.2 22.0 %copy-start.75 = (f32[64,2]{0,1:T(2,128)S(1)}, f32[64,2]{0,1:T(2,128)}, u32[]{:S(2)}) copy-start(f32[64,2]{0,1:T(2,128)} %param.31) | copy-start | bytes 1540
  481.2 40.0 %all-to-all-start.3 = ((bf16[64,2,2,2048]{3,2,1,0:T(2,128)(2,1)}), bf16[64,2,2,2048]{3,2,1,0:T(2,128)(2,1)}, u32[]{:S(2)}, u32[]{:S(2)}) async-start(bf16[64,2,2,2048]{3,2,1,0:T(2,128)(2,1)} %copy.289), calls=%async_computation.3 | async-start | bytes 2097152 | tf_op jit(solution)/shard_map/all_to_all | solution.py:299
  (37 other events, 65.5 us)
Sparse Core Ops, SparseCore 0:
  176.9 38.2 all-gather.14
  332.0 45.6 all-gather.12
  405.2 34.8 all-gather.10
where the time goes:
time: 542 us; the launch traced here: 536 us
  waiting for transfers between devices  142 us (26%)
  matrix products  123 us (23%)
  local copies, waits for them, and re-layouts  104 us (19%)
  blocking collectives  58 us (11%)
  between operations  55 us (10%)
  starting transfers between devices  29.2 us (5%)
  other arithmetic  25.1 us (5%)
    all_gather x1, waiting for transfers between devices, per_device(): lax.all_gather(arrived[None], 'tp', axis=0, tiled=True)  45.8 us
    all_to_all x1, blocking collectives, per_device(): lax.all_to_all(outgoing.reshape(groups, EXP_DEV, capacity, model_width),...  42.3 us
    dot_general x15, matrix products, apply_scores(): return jnp.einsum('bhts,bhsn->bhtn', scores, operand, precision=highest)  37 us
    all_gather x1, waiting for transfers between devices, per_device(): lax.all_gather(stream, 'tp', axis=0, tiled=True)  36.8 us
    all_to_all x1, waiting for transfers between devices, per_device(): lax.all_to_all(expert_sum[0].astype(jnp.bfloat16), SP, split_axis=0, conc...  27 us
    all_to_all x3, waiting for transfers between devices, sent_and_summed(): lax.all_to_all(pieces, axis, split_axis=0, concat_axis=0, tiled=True)  26.4 us
    dot_general x17, matrix products, link_states(): jnp.einsum('hij,hjk->hik', add_one, map_two, precision=highest)  17.7 us
    reshape x18, local copies, waits for them, and re-layouts, all_in_one(): jnp.pad(leaves[k].reshape(-1), (0, -leaves[k].size % width))  17.2 us
  transfers between devices with their start and end apart: 7, of which 7 were waited for; matrix products, arithmetic and copies ran while one was open for 9% of the time, Pallas kernels for 0%

commit v1 on v0

--- a/solution.py
+++ b/solution.py
@@ -16,6 +16,28 @@
 norm_eps = 1e-05
 unit_eps = 1e-06
 highest = lax.Precision.HIGHEST
+
+
+def joined_along(blocks, dim):
+    blocks = jnp.moveaxis(blocks, 0, dim)
+    lengths = blocks.shape
+    return blocks.reshape(*lengths[:dim], lengths[dim] * lengths[dim + 1], *lengths[dim + 2 :])
+
+
+def gather_around(x, axis, dim):
+    size = lax.axis_size(axis)
+    pairs = [(i, (i + 1) % size) for i in range(size)]
+    back = [(b, a) for a, b in pairs]
+    lower, upper = ([], [])
+    for turn in range(size - 1):
+        if turn % 2 == 0:
+            lower.append(lax.ppermute(lower[-1] if lower else x, axis, pairs))
+        else:
+            upper.append(lax.ppermute(upper[-1] if upper else x, axis, back))
+    blocks = jnp.stack([*lower[::-1], x, *upper])
+    shift = lax.axis_index(axis) - len(lower)
+    blocks = blocks[(jnp.arange(size) - shift) % size]
+    return joined_along(blocks, dim)
 
 
 def filled_with(x, identity):
@@ -276,7 +298,7 @@
     )
     arrived_all, rows_all = (
         lax.all_gather(arrived[None], "tp", axis=0, tiled=True),
-        lax.all_gather(stream, "tp", axis=0, tiled=True),
+        gather_around(stream, "tp", 0),
     )
     gated = jnp.einsum(
         "qsecd,edf->qsecf", arrived_all, routed_gate_weight, preferred_element_type=jnp.float32

time: 542 us -> 537 us (level)
  matrix products: 123 us -> 111 us
    ppermute x0 -> x3, waiting for transfers between devices: none -> 57.7 us  [the longest x2 57.7 us: gather_around(): lower.append(lax.ppermute(lower[-1] if lower else x, axis, pairs))]
    all_gather x1 -> x0, waiting for transfers between devices: 36.8 us -> none  [per_device(): lax.all_gather(stream, 'tp', axis=0, tiled=True)]
    all_to_all x3, waiting for transfers between devices: 26.4 us -> 10.2 us  [sent_and_summed(): lax.all_to_all(pieces, axis, split_axis=0, concat_axis=0, tiled=True)]
    dot_general x15, matrix products: 37 us -> 25.8 us  [apply_scores(): return jnp.einsum('bhts,bhsn->bhtn', scores, operand, precision=highest)]
  transfers between devices with their start and end apart: 7 -> 9, of which waited for: 7 -> 7; matrix products, arithmetic and copies ran while one was open for 9% -> 10% of each run, Pallas kernels for 0% -> 0%
where the time goes in v1:
time: 537 us; the launch traced here: 531 us
  waiting for transfers between devices  146 us (27%)
  matrix products  111 us (21%)
  local copies, waits for them, and re-layouts  106 us (20%)
  blocking collectives  58 us (11%)
  between operations  54 us (10%)
  starting transfers between devices  29.4 us (5%)
  other arithmetic  26 us (5%)
    ppermute x2, waiting for transfers between devices, gather_around(): lower.append(lax.ppermute(lower[-1] if lower else x, axis, pairs))  57.7 us
    all_gather x1, waiting for transfers between devices, per_device(): lax.all_gather(arrived[None], 'tp', axis=0, tiled=True)  45.8 us
    all_to_all x1, blocking collectives, per_device(): lax.all_to_all(outgoing.reshape(groups, EXP_DEV, capacity, model_width),...  42.5 us
    all_to_all x1, waiting for transfers between devices, per_device(): lax.all_to_all(expert_sum[0].astype(jnp.bfloat16), SP, split_axis=0, conc...  27 us
    dot_general x15, matrix products, apply_scores(): return jnp.einsum('bhts,bhsn->bhtn', scores, operand, precision=highest)  25.8 us
    dot_general x17, matrix products, link_states(): jnp.einsum('hij,hjk->hik', add_one, map_two, precision=highest)  17.8 us
    reshape x18, local copies, waits for them, and re-layouts, all_in_one(): jnp.pad(leaves[k].reshape(-1), (0, -leaves[k].size % width))  17.4 us
    convert_element_type x14, local copies, waits for them, and re-layouts, prefix_by_axis(): part[k].astype(own.dtype)  16.3 us
  transfers between devices with their start and end apart: 9, of which 7 were waited for; matrix products, arithmetic and copies ran while one was open for 10% of the time, Pallas kernels for 0%

profile of v1, /device:TPU:1, one launch (start us, length us, event | category | flops | bytes accessed | tf_op | source)
XLA Modules:
  0.0 531.0 jit_solution(15452122540909762920)
XLA Ops:
  14.5 2.3 reshape.550
  22.5 3.1 convolution_multiply_fusion.1
  25.6 2.2 fusion.17
  36.7 2.2 fusion.192
  39.0 2.2 convolution_add_fusion.1
  42.5 3.2 convolution_add_fusion
  49.4 3.0 convolution_add_fusion.5
  52.4 2.5 convolution_add_fusion.6
  60.7 2.1 convolution_convert_fusion.2
  70.5 5.0 all-gather.4
  91.5 2.0 convolution_add_fusion.12
  96.0 2.1 fusion.184
  99.1 2.0 fusion.183
  104.3 10.4 %all-gather.5 = bf16[4,1026,64]{1,2,0:T(8,128)(2,1)S(1)} all-gather(bf16[1,1026,64]{1,2,0:T(8,128)(2,1)} %bitcast.431), channel_id=3, replica_groups=mesh['sp_0'=8,'sp_1'=4,'sp_2'=2,'tp'=4] {'sp_1'}, dimensions={0}, use_global_device_ids=true | all-gather | bytes 656640 | tf_op jit(solution)/shard_map/all_gather | solution.py:57
  135.0 1.9 fusion.131
  136.9 2.0 convolution_add_fusion.11
  152.1 2.0 fusion.186
  159.0 1.9 fusion.185
  164.1 2.1 reshape.631
  166.3 4.2 fusion.18
  170.5 3.4 convolution_multiply_fusion
  173.9 3.1 fusion.80
  184.1 2.3 convolution_bitcast_fusion.2
  186.4 2.6 convolution_add_fusion.8
  196.9 5.6 %all-gather.12.cloned.1.call-done = bf16[8,1026,64]{1,2,0:T(8,128)(2,1)} async-done(((bf16[1,1026,64]{1,2,0:T(8,128)(2,1)}), bf16[8,1026,64]{1,2,0:T(8,128)(2,1)}) %all-gather.12.cloned.1.call-update) | async-done | bytes 1050640 | tf_op jit(solution)/shard_map/all_gather | solution.py:57
  224.3 2.2 fusion.174
  246.6 3.1 fusion.187
  253.2 3.3 convolution_convert_fusion.1
  256.5 4.1 all-to-all-start
  261.8 1.9 reduce_window_sum.23
  264.9 5.5 %all-to-all-done = bf16[4,64,2048]{2,1,0:T(8,128)(2,1)S(1)} async-done(((bf16[4,64,2048]{2,1,0:T(8,128)(2,1)}), bf16[4,64,2048]{2,1,0:T(8,128)(2,1)S(1)}, u32[]{:S(2)}, u32[]{:S(2)}) %all-to-all-start) | async-done | bytes 1048608 | tf_op jit(solution)/shard_map/all_to_all | solution.py:98
  272.8 2.2 scatter_custom_fusion
  276.5 42.5 %all_to_all.25 = bf16[64,2,2,2048]{3,2,1,0:T(2,128)(2,1)} all-to-all(bf16[64,2,2,2048]{3,2,1,0:T(2,128)(2,1)} %reshape.583), channel_id=1, replica_groups=mesh['sp_0'=8,'sp_1'=4,'sp_2'=2,'tp'=4] {'sp_0','sp_1','sp_2'}, dimensions={0} | all-to-all | bytes 2097152 | tf_op jit(solution)/shard_map/all_to_all | solution.py:292
  319.1 45.8 %all-gather.10.cloned.1.call-done = bf16[256,2,2,2048]{3,2,1,0:T(2,128)(2,1)} async-done(((bf16[64,2,2,2048]{3,2,1,0:T(2,128)(2,1)}), bf16[256,2,2,2048]{3,2,1,0:T(2,128)(2,1)}) %all-gather.10.cloned.1.call-update) | async-done | bytes 4194320 | tf_op jit(solution)/shard_map/all_gather | solution.py:300
  364.8 4.6 copy.284
  369.5 2.0 copy-done.14
  372.7 7.3 %convert_bitcast_fusion = bf16[4,1,64,2,2,2048]{5,2,4,0,3,1:T(8,128)(2,1)} fusion(bf16[2,256,2048]{2,1,0:T(8,128)(2,1)S(1)} %copy-done, bf16[2,2048,256]{2,1,0:T(8,128)(2,1)} %param.33, bf16[4,64,2,2,2048]{4,1,0,3,2:T(8,128)(2,1)} %bitcast.401, f32[4,64,2,2,256]{4,1,3,0,2:T(8,128)S(1)} %fusion.7), kind=kOutput, calls=%fused_computation.3 | convolution fusion | flops 2151153664 | bytes 13631488 | tf_op jit(solution)/shard_map/qsecf,efd->qsecd/dot_general | solution.py:310
  380.1 4.8 copy.287
  384.8 4.9 all-to-all-start.2
  392.7 50.4 %collective-permute-done = bf16[64,2048]{1,0:T(8,128)(2,1)S(1)} collective-permute-done((bf16[64,2048]{1,0:T(8,128)(2,1)S(1)}, bf16[64,2048]{1,0:T(8,128)(2,1)S(1)}, u32[]{:S(2)}, u32[]{:S(2)}) %collective-permute-start) | collective-permute-done | bytes 262176 | tf_op jit(solution)/shard_map/ppermute | solution.py:34
  443.1 7.3 %collective-permute-done.1 = bf16[64,2048]{1,0:T(8,128)(2,1)S(1)} collective-permute-done((bf16[64,2048]{1,0:T(8,128)(2,1)S(1)}, bf16[64,2048]{1,0:T(8,128)(2,1)S(1)}, u32[]{:S(2)}, u32[]{:S(2)}) %collective-permute-start.1) | collective-permute-done | bytes 262176 | tf_op jit(solution)/shard_map/ppermute | solution.py:34
  454.9 2.9 convolution_convert_fusion
  457.8 3.5 all-to-all-start.4
  461.3 4.3 reduce_sum.100
  465.6 3.3 copy.289
  469.0 4.7 all-to-all-done.4
  473.6 13.9 %all-to-all-start.3 = ((bf16[64,2,2,2048]{3,2,1,0:T(2,128)(2,1)}), bf16[64,2,2,2048]{3,2,1,0:T(2,128)(2,1)}, u32[]{:S(2)}, u32[]{:S(2)}) async-start(bf16[64,2,2,2048]{3,2,1,0:T(2,128)(2,1)} %copy.289), calls=%async_computation.3 | async-start | bytes 2097152 | tf_op jit(solution)/shard_map/all_to_all | solution.py:321
  488.6 27.0 %all-to-all-done.3 = bf16[64,2,2,2048]{3,2,1,0:T(2,128)(2,1)} async-done(((bf16[64,2,2,2048]{3,2,1,0:T(2,128)(2,1)}), bf16[64,2,2,2048]{3,2,1,0:T(2,128)(2,1)}, u32[]{:S(2)}, u32[]{:S(2)}) %all-to-all-start.3) | async-done | bytes 1048608 | tf_op jit(solution)/shard_map/all_to_all | solution.py:321
  (325 shorter events, 150.1 us)
Async XLA Ops:
  6.5 366.2 %copy-start = (bf16[2,256,2048]{2,1,0:T(8,128)(2,1)S(1)}, bf16[2,256,2048]{2,1,0:T(8,128)(2,1)}, u32[]{:S(2)}) copy-start(bf16[2,256,2048]{2,1,0:T(8,128)(2,1)} %param.34) | copy-start | bytes 6291460
  6.5 6.6 %copy-start.68 = (bf16[256,8]{0,1:T(8,128)(2,1)S(1)}, bf16[256,8]{0,1:T(8,128)(2,1)}, u32[]{:S(2)}) copy-start(bf16[256,8]{0,1:T(8,128)(2,1)} %param.23) | copy-start | bytes 12292
  6.5 6.8 %copy-start.54 = (bf16[256,512]{1,0:T(8,128)(2,1)S(1)}, bf16[256,512]{1,0:T(8,128)(2,1)}, u32[]{:S(2)}) copy-start(bf16[256,512]{1,0:T(8,128)(2,1)} %param.22) | copy-start | bytes 786436
  6.5 196.0 %all-gather.12.cloned.1.call-start = ((), (), s32[]{:S(2)}) async-start(), calls=%async_computation.6 | async-start | bytes 1327104 | tf_op jit(solution)/shard_map/all_gather | solution.py:57
  12.8 4.1 copy-start.1
  12.8 4.0 copy-start.67
  16.9 3.9 copy-start.10
  42.2 3.5 copy-start.12
  42.2 3.5 copy-start.16
  54.9 3.8 copy-start.11
  55.2 3.4 copy-start.18
  166.3 4.2 copy-start.4
  166.3 4.2 copy-start.7
  166.3 4.2 copy-start.40
  170.5 3.4 copy-start.6
  178.6 5.4 %copy-start.17 = (f32[8,64,64]{2,1,0:T(8,128)S(1)}, f32[8,64,64]{2,1,0:T(8,128)}, u32[]{:S(2)}) copy-start(f32[8,64,64]{2,1,0:T(8,128)} %fusion.118) | copy-start | bytes 393220
  178.6 7.8 %copy-start.13 = (bf16[4,64,8,64]{3,2,1,0:T(8,128)(2,1)S(1)}, bf16[4,64,8,64]{3,2,1,0:T(8,128)(2,1)}, u32[]{:S(2)}) copy-start(bf16[4,64,8,64]{3,2,1,0:T(8,128)(2,1)} %reshape.554) | copy-start | bytes 786436
  184.1 5.0 copy-start.9
  186.4 3.9 copy-start.28
  186.4 5.2 copy-start.38
  189.1 3.9 copy-start.26
  189.1 5.1 copy-start.39
  189.1 5.1 copy-start.44
  190.3 4.2 copy-start.21
  190.3 4.2 copy-start.24
  190.3 4.3 copy-start.31
  190.4 4.3 copy-start.46
  191.6 4.1 copy-start.29
  191.6 4.1 copy-start.33
  191.6 4.1 copy-start.36
  191.6 4.1 copy-start.47
  240.1 3.8 copy-start.50
  240.1 4.1 copy-start.51
  240.1 4.3 copy-start.52
  241.4 3.3 copy-start.41
  253.2 7.4 %copy-start.70 = (s32[256,2]{0,1:T(2,128)S(1)}, s32[256,2]{0,1:T(2,128)}, u32[]{:S(2)}) copy-start(s32[256,2]{0,1:T(2,128)} %param.30) | copy-start | bytes 6148
  256.5 14.0 %copy-start.22 = (bf16[64,2048]{1,0:T(8,128)(2,1)S(1)}, bf16[64,2048]{1,0:T(8,128)(2,1)}, u32[]{:S(2)}) copy-start(bf16[64,2048]{1,0:T(8,128)(2,1)} %param.26) | copy-start | bytes 786436
  256.5 13.8 %all-to-all-start = ((bf16[4,64,2048]{2,1,0:T(8,128)(2,1)}), bf16[4,64,2048]{2,1,0:T(8,128)(2,1)S(1)}, u32[]{:S(2)}, u32[]{:S(2)}) async-start(bf16[4,64,2048]{2,1,0:T(8,128)(2,1)} %bitcast.123), calls=%async_computation | async-start | bytes 2097152 | tf_op jit(solution)/shard_map/all_to_all | solution.py:98
  260.6 104.2 %all-gather.10.cloned.1.call-start = ((), (), s32[]{:S(2)}) async-start(), calls=%async_computation.5 | async-start | bytes 5242880 | tf_op jit(solution)/shard_map/all_gather | solution.py:300
  260.9 10.0 %copy-start.66 = (f32[2048]{0:T(1024)S(1)}, f32[2048]{0:T(1024)}, u32[]{:S(2)}) copy-start(f32[2048]{0:T(1024)} %param.29) | copy-start | bytes 24580
  364.8 6.6 %copy-start.74 = (bf16[2,2048,256]{2,1,0:T(8,128)(2,1)S(1)}, bf16[2,2048,256]{2,1,0:T(8,128)(2,1)}, u32[]{:S(2)}) copy-start(bf16[2,2048,256]{2,1,0:T(8,128)(2,1)} %param.32) | copy-start | bytes 6291460
  384.8 73.0 %all-to-all-start.2 = ((bf16[4,1,64,2,2,2048]{5,2,4,3,1,0:T(8,128)(2,1)}), bf16[4,1,64,2,2,2048]{5,2,4,3,1,0:T(8,128)(2,1)}, u32[]{:S(2)}, u32[]{:S(2)}) async-start(bf16[4,1,64,2,2,2048]{5,2,4,3,1,0:T(8,128)(2,1)} %copy.287), calls=%async_computation.2 | async-start | bytes 8388608 | tf_op jit(solution)/shard_map/all_to_all | solution.py:98
  389.7 53.3 %collective-permute-start = (bf16[64,2048]{1,0:T(8,128)(2,1)S(1)}, bf16[64,2048]{1,0:T(8,128)(2,1)S(1)}, u32[]{:S(2)}, u32[]{:S(2)}) collective-permute-start(bf16[64,2048]{1,0:T(8,128)(2,1)S(1)} %multiply_convert_fusion), channel_id=1, source_target_pairs={{0,1},{1,2},{2,3},{3,0},{4,5},{5,6},{6,7},{7,4},{8,9},{9,10},{10,1... | collective-permute-start | bytes 786440 | tf_op jit(solution)/shard_map/ppermute | solution.py:34
  391.3 51.8 %collective-permute-start.2 = (bf16[64,2048]{1,0:T(8,128)(2,1)S(1)}, bf16[64,2048]{1,0:T(8,128)(2,1)S(1)}, u32[]{:S(2)}, u32[]{:S(2)}) collective-permute-start(bf16[64,2048]{1,0:T(8,128)(2,1)S(1)} %multiply_convert_fusion), channel_id=1, source_target_pairs={{1,0},{2,1},{3,2},{0,3},{5,4},{6,5},{7,6},{4,7},{9,8},{10,9},{11,1... | collective-permute-start | bytes 786440 | tf_op jit(solution)/shard_map/ppermute | solution.py:36
  443.1 7.4 %collective-permute-start.1 = (bf16[64,2048]{1,0:T(8,128)(2,1)S(1)}, bf16[64,2048]{1,0:T(8,128)(2,1)S(1)}, u32[]{:S(2)}, u32[]{:S(2)}) collective-permute-start(bf16[64,2048]{1,0:T(8,128)(2,1)S(1)} %collective-permute-done), channel_id=1, source_target_pairs={{0,1},{1,2},{2,3},{3,0},{4,5},{5,6},{6,7},{7,4},{8,9},{9,10},{10,1... | collective-permute-start | bytes 786440 | tf_op jit(solution)/shard_map/ppermute | solution.py:34
  457.8 15.8 %all-to-all-start.4 = ((bf16[4,64,2048]{2,1,0:T(8,128)(2,1)}), bf16[4,64,2048]{2,1,0:T(8,128)(2,1)S(1)}, u32[]{:S(2)}, u32[]{:S(2)}) async-start(bf16[4,64,2048]{2,1,0:T(8,128)(2,1)} %bitcast.399), calls=%async_computation.4 | async-start | bytes 2097152 | tf_op jit(solution)/shard_map/all_to_all | solution.py:98
  465.6 21.9 %copy-start.72 = (f32[64,2]{0,1:T(2,128)S(1)}, f32[64,2]{0,1:T(2,128)}, u32[]{:S(2)}) copy-start(f32[64,2]{0,1:T(2,128)} %param.31) | copy-start | bytes 1540
  473.6 42.0 %all-to-all-start.3 = ((bf16[64,2,2,2048]{3,2,1,0:T(2,128)(2,1)}), bf16[64,2,2,2048]{3,2,1,0:T(2,128)(2,1)}, u32[]{:S(2)}, u32[]{:S(2)}) async-start(bf16[64,2,2,2048]{3,2,1,0:T(2,128)(2,1)} %copy.289), calls=%async_computation.3 | async-start | bytes 2097152 | tf_op jit(solution)/shard_map/all_to_all | solution.py:321
  (36 other events, 63.8 us)
Sparse Core Ops, SparseCore 0:
  164.3 38.2 all-gather.11
  319.2 45.6 all-gather.9
